TPU v7x, 32 devices: a whole 2x2x4 slice. The times are simulated.
32 devices in a mesh: ep: 8 (over z, core), tp: 4 (over y, x).
Axes of the slice: x: 2, y: 2, z: 4, core: 2. Of those that a mesh axis runs over, the one named last changes fastest.
Arguments:
- tokens: bfloat16 [1024, 2048], P('ep'), may hold values from -6 to 6
- cotangent: bfloat16 [1024, 2048], P('ep'), may hold values from -6 to 6
- routes: int32 [1024, 2], P('ep'), may hold values from 0 to 7, all different within a row; in each aligned block of 128 rows (0 to 127, 128 to 255, ...) at most 64 rows name the same one
- route_weight: float32 [1024, 2], P('ep'), may hold values from 0.1 to 1
- w_gate: bfloat16 [8, 2048, 1024], P('ep', None, 'tp'), may hold values from -0.1875 to 0.1875
- w_up: bfloat16 [8, 2048, 1024], P('ep', None, 'tp'), may hold values from -0.1875 to 0.1875
- w_down: bfloat16 [8, 1024, 2048], P('ep', 'tp'), may hold values from -0.1875 to 0.1875
Outputs:
- grad_tokens: bfloat16 [1024, 2048], P('ep', 'tp')
- grad_route_weight: float32 [1024, 2], P('ep')
- grad_gate: float32 [8, 2048, 1024], P('ep', None, 'tp')
- grad_up: float32 [8, 2048, 1024], P('ep', None, 'tp')
- grad_down: float32 [8, 1024, 2048], P('ep', 'tp')
Inputs may be any that keep to these rules, and one draw needn't show every extreme that they name: `routes`: each row names 2 different experts. In each aligned block of 128 rows (the rows of one index of ep) no expert is named by more than 64 rows, and in every draw some expert is named by exactly 64 rows of some block.
All inputs are finite; a program needn't handle non-finite values.
Results may differ from a plain program's by a relative error of at most 0.023.
Values may be sent and summed in bfloat16 or wider, within the bound.
A program may use at most 64 MiB of HBM per device.

v0:
```python
import jax
import jax.numpy as jnp
from jax import lax
from jax.sharding import PartitionSpec as P


def slot_index(block_routes, experts, capacity):
    flat_ids = block_routes.reshape(-1)
    onehot = (flat_ids[:, None] == jnp.arange(experts, dtype=jnp.int32)[None, :]).astype(jnp.int32)
    earlier = jnp.cumsum(onehot, axis=0) - onehot
    return flat_ids * capacity + jnp.sum(earlier * onehot, axis=1)


def on_device(tokens, cotangent, routes, route_weight, w_gate, w_up, w_down):
    f32 = jnp.float32
    tok_rows, model_width = tokens.shape
    choices_row = routes.shape[1]
    experts = lax.axis_size("ep")
    capacity = 2 * tok_rows * choices_row // experts
    recv_rows = experts * capacity
    slot_ids = slot_index(routes, experts, capacity)
    send_w = jnp.zeros((recv_rows,), f32).at[slot_ids].set(route_weight.reshape(-1))
    send_x = (
        jnp.zeros((recv_rows, model_width), jnp.bfloat16)
        .at[slot_ids]
        .set(jnp.repeat(tokens, choices_row, axis=0))
    )
    send_dy = (
        jnp.zeros((recv_rows, model_width), jnp.bfloat16)
        .at[slot_ids]
        .set(jnp.repeat(cotangent, choices_row, axis=0))
    )
    got_x = lax.all_to_all(
        send_x.reshape(experts, capacity, model_width),
        "ep",
        split_axis=0,
        concat_axis=0,
        tiled=True,
    )
    got_dy, got_w = (
        lax.all_to_all(
            send_dy.reshape(experts, capacity, model_width),
            "ep",
            split_axis=0,
            concat_axis=0,
            tiled=True,
        ),
        lax.all_to_all(
            send_w.reshape(experts, capacity, 1).astype(jnp.bfloat16),
            "ep",
            split_axis=0,
            concat_axis=0,
            tiled=True,
        ).astype(jnp.float32),
    )
    rows_x = got_x.reshape(recv_rows, model_width)
    rows_dy = got_dy.reshape(recv_rows, model_width)
    rows_w = got_w.reshape(recv_rows)
    gate_w = w_gate[0]
    up_w = w_up[0]
    down_w = w_down[0]
    gate_pre = jnp.dot(rows_x, gate_w, preferred_element_type=f32)
    up_pre = jnp.dot(rows_x, up_w, preferred_element_type=f32)
    gate_sig = jax.nn.sigmoid(gate_pre)
    act_full = gate_pre * gate_sig * up_pre
    act = act_full.astype(jnp.bfloat16)
    back_hidden = jnp.einsum("rd,fd->rf", rows_dy, down_w, preferred_element_type=f32)
    weighted_cot = (rows_w[:, None] * rows_dy.astype(f32)).astype(jnp.bfloat16)
    d_hidden = rows_w[:, None] * back_hidden
    d_gate = (d_hidden * up_pre * gate_sig * (1.0 + gate_pre * (1.0 - gate_sig))).astype(
        jnp.bfloat16
    )
    d_up = (d_hidden * gate_pre * gate_sig).astype(jnp.bfloat16)
    gate_part = jnp.sum(act_full * back_hidden, axis=1)
    token_part = jnp.einsum("rf,df->rd", d_gate, gate_w, preferred_element_type=f32)
    token_part = token_part + jnp.einsum("rf,df->rd", d_up, up_w, preferred_element_type=f32)
    grad_gate = jnp.einsum("rd,rf->df", rows_x, d_gate, preferred_element_type=f32)[None]
    grad_up = jnp.einsum("rd,rf->df", rows_x, d_up, preferred_element_type=f32)[None]
    grad_down = jnp.einsum("rf,rd->fd", act, weighted_cot, preferred_element_type=f32)[None]
    rounded_part = token_part.astype(jnp.bfloat16).astype(f32)
    shares = lax.psum_scatter(
        rounded_part.astype(jnp.bfloat16), "tp", scatter_dimension=1, tiled=True
    )
    gate_total = lax.psum(gate_part, "tp")
    back_x, back_gate = (
        lax.all_to_all(
            shares.reshape(experts, capacity, -1), "ep", split_axis=0, concat_axis=0, tiled=True
        ),
        lax.all_to_all(
            gate_total.reshape(experts, capacity).astype(jnp.bfloat16),
            "ep",
            split_axis=0,
            concat_axis=0,
            tiled=True,
        ).astype(jnp.float32),
    )
    picked = back_x.reshape(recv_rows, -1)[slot_ids].astype(f32).reshape(tok_rows, choices_row, -1)
    grad_route_weight = back_gate.reshape(recv_rows)[slot_ids].reshape(tok_rows, choices_row)
    grad_tokens = jnp.sum(picked, axis=1).astype(jnp.bfloat16)
    return (grad_tokens, grad_route_weight, grad_gate, grad_up, grad_down)


def solution(mesh):
    return jax.shard_map(
        on_device,
        mesh=mesh,
        in_specs=(
            P("ep", None),
            P("ep", None),
            P("ep", None),
            P("ep", None),
            P("ep", None, "tp"),
            P("ep", None, "tp"),
            P("ep", "tp", None),
        ),
        out_specs=(
            P("ep", "tp"),
            P("ep", None),
            P("ep", None, "tp"),
            P("ep", None, "tp"),
            P("ep", "tp", None),
        ),
        check_vma=False,
    )
```

profile of v0, /device:TPU:0, one launch (start us, length us, event | category | flops | bytes accessed | tf_op | source)
XLA Modules:
  0.0 204.4 jit_solution(6226515418435991315)
XLA Ops:
  13.2 6.4 %all-to-all-start = ((bf16[8,64,1]{1,2,0:T(2,128)(2,1)}), bf16[8,64,1]{1,2,0:T(2,128)(2,1)S(1)}, u32[]{:S(2)}, u32[]{:S(2)}) async-start(bf16[8,64,1]{1,2,0:T(2,128)(2,1)} %convert_element_type.80), calls=%async_computation | async-start | bytes 8192 | tf_op jit(solution)/shard_map/all_to_all | solution.py:48
  19.6 1.7 broadcast_in_dim.26
  21.7 3.7 %scatter_custom_fusion.2 = bf16[512,2048]{1,0:T(8,128)(2,1)} fusion(s32[256]{0:T(256)S(1)} %bitcast.54, bf16[256,2048]{1,0:T(8,128)(2,1)S(1)} %reshape.170, bf16[]{:T(256)} %constant.5.clone.1), kind=kCustom, calls=%fused_computation.20 | custom fusion | bytes 2097154 | tf_op jit(solution)/shard_map/scatter | solution.py:26
  25.4 5.1 %all-to-all-start.2 = ((bf16[8,64,2048]{2,1,0:T(8,128)(2,1)}), bf16[8,64,2048]{2,1,0:T(8,128)(2,1)S(1)}, u32[]{:S(2)}, u32[]{:S(2)}) async-start(bf16[8,64,2048]{2,1,0:T(8,128)(2,1)} %bitcast.51), calls=%async_computation.2 | async-start | bytes 4194304 | tf_op jit(solution)/shard_map/all_to_all | solution.py:33
  30.5 2.6 %broadcast_in_dim.25 = bf16[128,2,2048]{2,1,0:T(2,128)(2,1)} broadcast(bf16[128,2048]{1,0:T(8,128)(2,1)} %param.8), dimensions={0,2} | broadcast | bytes 1572864 | tf_op jit(solution)/shard_map/broadcast_in_dim | solution.py:31
  33.2 2.2 %reshape.162 = bf16[256,2048]{1,0:T(8,128)(2,1)} reshape(bf16[128,2,2048]{2,1,0:T(2,128)(2,1)} %broadcast_in_dim.25) | data formatting | bytes 2097152 | tf_op jit(solution)/shard_map/reshape | solution.py:31
  35.4 4.4 %scatter_custom_fusion.1 = bf16[512,2048]{1,0:T(8,128)(2,1)} fusion(s32[256]{0:T(256)S(1)} %bitcast.55, bf16[256,2048]{1,0:T(8,128)(2,1)} %reshape.162, bf16[]{:T(256)} %constant.5.clone.1), kind=kCustom, calls=%fused_computation.22 | custom fusion | bytes 2097664 | tf_op jit(solution)/shard_map/scatter | solution.py:31
  39.8 39.8 %all-to-all-done.2 = bf16[8,64,2048]{2,1,0:T(8,128)(2,1)S(1)} async-done(((bf16[8,64,2048]{2,1,0:T(8,128)(2,1)}), bf16[8,64,2048]{2,1,0:T(8,128)(2,1)S(1)}, u32[]{:S(2)}, u32[]{:S(2)}) %all-to-all-start.2) | async-done | bytes 2097184 | tf_op jit(solution)/shard_map/all_to_all | solution.py:33
  79.6 4.3 %all-to-all-start.1 = ((bf16[8,64,2048]{2,1,0:T(8,128)(2,1)}), bf16[8,64,2048]{2,1,0:T(8,128)(2,1)}, u32[]{:S(2)}, u32[]{:S(2)}) async-start(bf16[8,64,2048]{2,1,0:T(8,128)(2,1)} %bitcast.50), calls=%async_computation.1 | async-start | bytes 4194304 | tf_op jit(solution)/shard_map/all_to_all | solution.py:41
  85.8 1.6 fusion.6
  87.4 45.6 %all-to-all-done.1 = bf16[8,64,2048]{2,1,0:T(8,128)(2,1)} async-done(((bf16[8,64,2048]{2,1,0:T(8,128)(2,1)}), bf16[8,64,2048]{2,1,0:T(8,128)(2,1)}, u32[]{:S(2)}, u32[]{:S(2)}) %all-to-all-start.1) | async-done | bytes 2097184 | tf_op jit(solution)/shard_map/all_to_all | solution.py:41
  132.9 3.1 %multiply_reduce_fusion = (f32[512]{0:T(512)S(1)}, bf16[512,256]{0,1:T(8,128)(2,1)S(1)}, bf16[512,256]{0,1:T(8,128)(2,1)S(1)}) fusion(f32[512,256]{0,1:T(8,128)} %fusion.6, f32[512,256]{0,1:T(8,128)} %fusion.3, f32[512]{0:T(512)S(1)} %reshape.132, bf16[512,2048]{1,0:T(8,128)(2,1)} %bitcast.5, bf16[1,256,2048]{2,1,0:T(8,128)(2,1)} %param.13), kind=kOutput, calls=%fused_computation.24 | convolution fusion | flops 539229696 | bytes 4722688 | tf_op jit(solution)/shard_map/rd,fd->rf/dot_general | solution.py:67
  137.4 2.1 %add_convert_fusion = bf16[512,2048]{1,0:T(8,128)(2,1)} fusion(f32[512,2048]{1,0:T(8,128)S(1)} %fusion.1, bf16[512,256]{0,1:T(8,128)(2,1)S(1)} %get-tuple-element.17, bf16[1,2048,256]{2,1,0:T(8,128)(2,1)S(1)} %copy-done.2), kind=kOutput, calls=%fused_computation.6 | convolution fusion | flops 538968064 | bytes 7602176 | tf_op jit(solution)/shard_map/rf,df->rd/dot_general | solution.py:76
  139.5 10.0 %psum.7 = bf16[512]{0:T(512)(128)(2,1)S(1)} all-reduce(f32[512]{0:T(512)S(1)} %get-tuple-element.15), channel_id=1, replica_groups=mesh['ep'=8,'tp'=4] {'tp'}, use_global_device_ids=true, to_apply=%region_9.10 | all-reduce | flops 512 | bytes 3072 | tf_op jit(solution)/shard_map/psum | solution.py:84
  150.2 3.3 %all-to-all-start.4 = ((bf16[8,1,64]{2,1,0:T(2,128)(2,1)}), bf16[8,1,64]{2,1,0:T(2,128)(2,1)S(1)}, u32[]{:S(2)}, u32[]{:S(2)}) async-start(bf16[8,1,64]{2,1,0:T(2,128)(2,1)} %convert_element_type.81), calls=%async_computation.5 | async-start | bytes 8192 | tf_op jit(solution)/shard_map/all_to_all | solution.py:89
  153.5 5.4 %all-to-all-done.4 = bf16[8,1,64]{2,1,0:T(2,128)(2,1)S(1)} async-done(((bf16[8,1,64]{2,1,0:T(2,128)(2,1)}), bf16[8,1,64]{2,1,0:T(2,128)(2,1)S(1)}, u32[]{:S(2)}, u32[]{:S(2)}) %all-to-all-start.4) | async-done | bytes 1056 | tf_op jit(solution)/shard_map/all_to_all | solution.py:89
  158.9 14.8 %reduce-scatter.2.cloned.1.call-done = bf16[512,512]{1,0:T(8,128)(2,1)} async-done(((bf16[512,2048]{1,0:T(8,128)(2,1)}), bf16[512,512]{1,0:T(8,128)(2,1)}) %reduce-scatter.2.cloned.1.call-update) | async-done | bytes 524304 | tf_op jit(solution)/shard_map/reduce_scatter | solution.py:81
  173.7 4.6 %all-to-all-start.3 = ((bf16[8,64,512]{2,1,0:T(8,128)(2,1)}), bf16[8,64,512]{2,1,0:T(8,128)(2,1)}, u32[]{:S(2)}, u32[]{:S(2)}) async-start(bf16[8,64,512]{2,1,0:T(8,128)(2,1)} %bitcast.52), calls=%async_computation.4 | async-start | bytes 1048576 | tf_op jit(solution)/shard_map/all_to_all | solution.py:86
  178.3 3.0 %convolution_bitcast_fusion.1 = f32[1,2048,256]{2,1,0:T(8,128)} fusion(bf16[512,2048]{1,0:T(8,128)(2,1)S(1)} %bitcast.48, bf16[512,256]{0,1:T(8,128)(2,1)} %copy-done.3), kind=kOutput, calls=%fused_computation.8 | convolution fusion | flops 536870912 | bytes 4456448 | tf_op jit(solution)/shard_map/rd,rf->df/dot_general | solution.py:78
  181.4 2.1 %convolution_bitcast_fusion.2 = f32[1,2048,256]{2,1,0:T(8,128)} fusion(bf16[512,2048]{1,0:T(8,128)(2,1)S(1)} %bitcast.49, bf16[512,256]{0,1:T(8,128)(2,1)S(1)} %get-tuple-element.16), kind=kOutput, calls=%fused_computation.9 | convolution fusion | flops 536870912 | bytes 4456448 | tf_op jit(solution)/shard_map/rd,rf->df/dot_general | solution.py:77
  183.5 3.8 %convolution_bitcast_fusion = f32[1,256,2048]{2,1,0:T(8,128)} fusion(bf16[512,2048]{1,0:T(8,128)(2,1)} %bitcast.5, f32[512]{0:T(512)S(1)} %reshape.132, f32[512,256]{0,1:T(8,128)S(1)} %copy-done.5, f32[512,256]{0,1:T(8,128)S(1)} %copy-done.4), kind=kOutput, calls=%fused_computation.7 | convolution fusion | flops 540803072 | bytes 5244928 | tf_op jit(solution)/shard_map/rf,rd->fd/dot_general | solution.py:79
  187.3 1.9 gather_fusion.1
  190.1 3.7 %all-to-all-done.3 = bf16[8,64,512]{2,1,0:T(8,128)(2,1)} async-done(((bf16[8,64,512]{2,1,0:T(8,128)(2,1)}), bf16[8,64,512]{2,1,0:T(8,128)(2,1)}, u32[]{:S(2)}, u32[]{:S(2)}) %all-to-all-start.3) | async-done | bytes 524320 | tf_op jit(solution)/shard_map/all_to_all | solution.py:86
  193.8 2.3 %gather_fusion = bf16[256,512]{1,0:T(8,128)(2,1)S(1)} fusion(bf16[512,512]{1,0:T(8,128)(2,1)} %bitcast.12, s32[1024]{0:T(1024)S(1)} %pad_clamp_fusion), kind=kCustom, calls=%fused_computation | custom fusion | bytes 525312 | tf_op jit(solution)/shard_map/gather | solution.py:97
  (46 shorter events, 12.7 us)
Async XLA Ops:
  7.2 77.1 %copy-start = (bf16[1,2048,256]{2,1,0:T(8,128)(2,1)S(1)}, bf16[1,2048,256]{2,1,0:T(8,128)(2,1)}, u32[]{:S(2)}) copy-start(bf16[1,2048,256]{2,1,0:T(8,128)(2,1)} %param.11) | copy-start | bytes 3145732
  13.2 12.2 %all-to-all-start = ((bf16[8,64,1]{1,2,0:T(2,128)(2,1)}), bf16[8,64,1]{1,2,0:T(2,128)(2,1)S(1)}, u32[]{:S(2)}, u32[]{:S(2)}) async-start(bf16[8,64,1]{1,2,0:T(2,128)(2,1)} %convert_element_type.80), calls=%async_computation | async-start | bytes 8192 | tf_op jit(solution)/shard_map/all_to_all | solution.py:48
  25.4 54.1 %all-to-all-start.2 = ((bf16[8,64,2048]{2,1,0:T(8,128)(2,1)}), bf16[8,64,2048]{2,1,0:T(8,128)(2,1)S(1)}, u32[]{:S(2)}, u32[]{:S(2)}) async-start(bf16[8,64,2048]{2,1,0:T(8,128)(2,1)} %bitcast.51), calls=%async_computation.2 | async-start | bytes 4194304 | tf_op jit(solution)/shard_map/all_to_all | solution.py:33
  79.6 53.4 %all-to-all-start.1 = ((bf16[8,64,2048]{2,1,0:T(8,128)(2,1)}), bf16[8,64,2048]{2,1,0:T(8,128)(2,1)}, u32[]{:S(2)}, u32[]{:S(2)}) async-start(bf16[8,64,2048]{2,1,0:T(8,128)(2,1)} %bitcast.50), calls=%async_computation.1 | async-start | bytes 4194304 | tf_op jit(solution)/shard_map/all_to_all | solution.py:41
  83.9 89.8 %reduce-scatter.2.cloned.1.call-start = ((), (), s32[]{:S(2)}) async-start(), calls=%async_computation.6 | async-start | bytes 2621440 | tf_op jit(solution)/shard_map/reduce_scatter | solution.py:81
  84.2 1.6 copy-start.1
  136.0 0.8 copy-start.3
  136.1 1.3 copy-start.2
  150.2 8.8 %all-to-all-start.4 = ((bf16[8,1,64]{2,1,0:T(2,128)(2,1)}), bf16[8,1,64]{2,1,0:T(2,128)(2,1)S(1)}, u32[]{:S(2)}, u32[]{:S(2)}) async-start(bf16[8,1,64]{2,1,0:T(2,128)(2,1)} %convert_element_type.81), calls=%async_computation.5 | async-start | bytes 8192 | tf_op jit(solution)/shard_map/all_to_all | solution.py:89
  173.7 20.0 %all-to-all-start.3 = ((bf16[8,64,512]{2,1,0:T(8,128)(2,1)}), bf16[8,64,512]{2,1,0:T(8,128)(2,1)}, u32[]{:S(2)}, u32[]{:S(2)}) async-start(bf16[8,64,512]{2,1,0:T(8,128)(2,1)} %bitcast.52), calls=%async_computation.4 | async-start | bytes 1048576 | tf_op jit(solution)/shard_map/all_to_all | solution.py:86
  181.4 2.1 %copy-start.4 = (f32[512,256]{0,1:T(8,128)S(1)}, f32[512,256]{0,1:T(8,128)}, u32[]{:S(2)}) copy-start(f32[512,256]{0,1:T(8,128)} %fusion.3) | copy-start | bytes 1572868
  181.4 2.1 %copy-start.5 = (f32[512,256]{0,1:T(8,128)S(1)}, f32[512,256]{0,1:T(8,128)}, u32[]{:S(2)}) copy-start(f32[512,256]{0,1:T(8,128)} %fusion.6) | copy-start | bytes 1572868
Sparse Core Ops, SparseCore 0:
  139.6 34.0 reduce-scatter.1
where the time goes:
time: 205 us; the launch traced here: 204 us
  waiting for transfers between devices  109 us (53%)
  local copies, waits for them, and re-layouts  26.3 us (13%)
  starting transfers between devices  23.9 us (12%)
  matrix products  18 us (9%)
  between operations  14.2 us (7%)
  blocking collectives  10 us (5%)
  other arithmetic  2.76 us (1%)
    all_to_all x1, waiting for transfers between devices, on_device(): lax.all_to_all(send_dy.reshape(experts, capacity, model_width), 'ep', spl...  45.6 us
    all_to_all x1, waiting for transfers between devices, on_device(): lax.all_to_all(send_x.reshape(experts, capacity, model_width), 'ep', spli...  39.8 us
    reduce_scatter x1, waiting for transfers between devices, on_device(): lax.psum_scatter(rounded_part.astype(jnp.bfloat16), 'tp', scatter_dimensi...  14.8 us
    psum x1, blocking collectives, on_device(): gate_total = lax.psum(gate_part, 'tp')  10 us
    all_to_all x1, starting transfers between devices, on_device(): lax.all_to_all(send_w.reshape(experts, capacity, 1).astype(jnp.bfloat16),...  6.35 us
    all_to_all x1, waiting for transfers between devices, on_device(): lax.all_to_all(gate_total.reshape(experts, capacity).astype(jnp.bfloat16)...  5.43 us
    all_to_all x1, starting transfers between devices, on_device(): lax.all_to_all(send_x.reshape(experts, capacity, model_width), 'ep', spli...  5.1 us
    all_to_all x1, starting transfers between devices, on_device(): lax.all_to_all(shares.reshape(experts, capacity, -1), 'ep', split_axis=0,...  4.61 us
  transfers between devices with their start and end apart: 6, of which 5 were waited for; matrix products, arithmetic and copies ran while one was open for 15% of the time, Pallas kernels for 0%

commit v1 on v0

--- a/solution.py
+++ b/solution.py
@@ -11,7 +11,7 @@
     return flat_ids * capacity + jnp.sum(earlier * onehot, axis=1)
 
 
-def on_device(tokens, cotangent, routes, route_weight, w_gate, w_up, w_down):
+def slotted(tokens, cotangent, routes, route_weight, w_gate, w_up, w_down):
     f32 = jnp.float32
     tok_rows, model_width = tokens.shape
     choices_row = routes.shape[1]
@@ -100,6 +100,48 @@
     return (grad_tokens, grad_route_weight, grad_gate, grad_up, grad_down)
 
 
+def dense(tokens, cotangent, routes, route_weight, w_gate, w_up, w_down):
+    f32, bf16 = jnp.float32, jnp.bfloat16
+    rows, width = tokens.shape
+    ep, tp = lax.axis_size("ep"), lax.axis_size("tp")
+    cols = width // tp
+    at = lax.axis_index("tp") * cols
+    mine = jnp.stack([lax.dynamic_slice_in_dim(a, at, cols, 1) for a in (tokens, cotangent)])
+    full = lax.all_gather(mine, ("ep", "tp"), tiled=False).reshape(ep, tp, 2, rows, cols)
+    full = full.transpose(2, 0, 3, 1, 4).reshape(2, ep * rows, width)
+    x, dy = full[0], full[1]
+    hit = routes[None] == jnp.arange(ep, dtype=routes.dtype)[:, None, None]
+    table = jnp.sum(jnp.where(hit, route_weight[None], 0.0), axis=2)
+    w = lax.all_to_all(table, "ep", split_axis=0, concat_axis=0, tiled=True).reshape(-1)[:, None]
+    g_w, u_w, d_w = w_gate[0], w_up[0], w_down[0]
+    g = jnp.dot(x, g_w, preferred_element_type=f32)
+    u = jnp.dot(x, u_w, preferred_element_type=f32)
+    back = jnp.einsum("rd,fd->rf", dy, d_w, preferred_element_type=f32)
+    sig = jax.nn.sigmoid(g)
+    act = g * sig * u
+    d_h = w * back
+    d_gate = (d_h * u * sig * (1.0 + g * (1.0 - sig))).astype(bf16)
+    d_up = (d_h * g * sig).astype(bf16)
+    part = jnp.sum(act * back, axis=1)
+    tok = jnp.einsum("rf,df->rd", d_gate, g_w, preferred_element_type=f32)
+    tok = tok + jnp.einsum("rf,df->rd", d_up, u_w, preferred_element_type=f32)
+    gg = jnp.einsum("rd,rf->df", x, d_gate, preferred_element_type=f32)[None]
+    gu = jnp.einsum("rd,rf->df", x, d_up, preferred_element_type=f32)[None]
+    gd = jnp.einsum("rf,rd->fd", (w * act).astype(bf16), dy, preferred_element_type=f32)[None]
+    share = lax.psum_scatter(tok.astype(bf16), "tp", scatter_dimension=1, tiled=True)
+    grad_tokens = lax.psum_scatter(share, "ep", scatter_dimension=0, tiled=True)
+    total = lax.psum(part, "tp").reshape(ep, rows)
+    home = lax.all_to_all(total, "ep", split_axis=0, concat_axis=0, tiled=True)
+    grw = jnp.sum(jnp.where(hit, home[:, :, None], 0.0), axis=0)
+    return grad_tokens, grw, gg, gu, gd
+
+
+def on_device(*args):
+    rows, width = args[0].shape
+    gathered = 4 * rows * width * lax.axis_size("ep")
+    return (dense if gathered <= 1 << 24 else slotted)(*args)
+
+
 def solution(mesh):
     return jax.shard_map(
         on_device,

time: 205 us -> 247 us (1.20)
  waiting for transfers between devices: 109 us -> 156 us
  starting transfers between devices: 23.9 us -> 0.3 us
  blocking collectives: 10 us -> 25.4 us
  matrix products: 18 us -> 22.1 us
    all_to_all x5 -> x0, waiting for transfers between devices: 94.4 us -> none  [the longest x1 45.6 us: on_device(): lax.all_to_all(send_dy.reshape(experts, capacity, model_width), 'ep', spl...]
    all_gather x0 -> x1, waiting for transfers between devices: none -> 82.2 us  [dense(): lax.all_gather(mine, ('ep', 'tp'), tiled=False)]
    reduce_scatter x1 -> x2, waiting for transfers between devices: 14.8 us -> 74.1 us  [the longest x1 49.7 us: dense(): lax.psum_scatter(tok.astype(bf16), 'tp', scatter_dimension=1, tiled=True)]
    all_to_all x5 -> x0, starting transfers between devices: 23.7 us -> none  [the longest x1 6.35 us: on_device(): lax.all_to_all(send_w.reshape(experts, capacity, 1).astype(jnp.bfloat16),...]
    slice x1 -> x3, local copies, waits for them, and re-layouts: 0.21 us -> 21.1 us  [dense(): x, dy = (full[0], full[1])]
    all_to_all x0 -> x2, blocking collectives: none -> 16.5 us  [the longest x1 8.6 us: dense(): home = lax.all_to_all(total, 'ep', split_axis=0, concat_axis=0, tiled=True)]
    scatter x3 -> x0, local copies, waits for them, and re-layouts: 9.51 us -> none  [the longest x1 4.4 us: on_device(): send_dy = jnp.zeros((recv_rows, model_width), jnp.bfloat16).at[slot_ids]....]
    gather x3 -> x0, local copies, waits for them, and re-layouts: 4.37 us -> none  [the longest x2 2.42 us: on_device(): back_x.reshape(recv_rows, -1)[slot_ids].astype(f32)]
  transfers between devices with their start and end apart: 6 -> 3, of which waited for: 5 -> 3; matrix products, arithmetic and copies ran while one was open for 15% -> 4% of each run, Pallas kernels for 0% -> 0%
where the time goes in v1:
time: 247 us
  waiting for transfers between devices  156 us (63%)
  blocking collectives  25.4 us (10%)
  local copies, waits for them, and re-layouts  25.2 us (10%)
  matrix products  22.1 us (9%)
  between operations  13.8 us (6%)
  other arithmetic  3.66 us (1%)
    all_gather x1, waiting for transfers between devices, dense(): lax.all_gather(mine, ('ep', 'tp'), tiled=False)  82.2 us
    reduce_scatter x1, waiting for transfers between devices, dense(): lax.psum_scatter(tok.astype(bf16), 'tp', scatter_dimension=1, tiled=True)  49.7 us
    reduce_scatter x1, waiting for transfers between devices, dense(): grad_tokens = lax.psum_scatter(share, 'ep', scatter_dimension=0, tiled=True)  24.3 us
    slice x3, local copies, waits for them, and re-layouts, dense(): x, dy = (full[0], full[1])  21.1 us
    psum x1, blocking collectives, dense(): total = lax.psum(part, 'tp').reshape(ep, rows)  8.9 us
    all_to_all x1, blocking collectives, dense(): home = lax.all_to_all(total, 'ep', split_axis=0, concat_axis=0, tiled=True)  8.6 us
    all_to_all x1, blocking collectives, dense(): lax.all_to_all(table, 'ep', split_axis=0, concat_axis=0, tiled=True)  7.94 us
    dot_general x1, matrix products, dense(): gu = jnp.einsum('rd,rf->df', x, d_up, preferred_element_type=f32)[None]  4.95 us
  transfers between devices with their start and end apart: 3, of which 3 were waited for; matrix products, arithmetic and copies ran while one was open for 4% of the time, Pallas kernels for 0%

profile of v1, /device:TPU:0, one launch (start us, length us, event | category | flops | bytes accessed | tf_op | source)
XLA Modules:
  0.0 246.8 jit_solution(3419523035908092545)
XLA Ops:
  7.2 1.1 dynamic-slice_bitcast_fusion
  8.3 0.7 pad_maximum_fusion
  9.1 82.2 %all-gather.3.cloned.1.call-done = bf16[64,128,512]{2,1,0:T(8,128)(2,1)} async-done(((bf16[2,128,512]{2,1,0:T(8,128)(2,1)}), bf16[64,128,512]{2,1,0:T(8,128)(2,1)}) %all-gather.3.cloned.1.call-update) | async-done | bytes 8388624 | tf_op jit(solution)/shard_map/all_gather | solution.py:110
  91.3 5.9 %fusion.34 = (bf16[1,8,128,4,512]{4,2,0,3,1:T(8,128)(2,1)}, bf16[1,8,128,4,512]{4,2,0,3,1:T(8,128)(2,1)}) fusion(bf16[2,8,128,4,512]{4,2,0,3,1:T(8,128)(2,1)} %bitcast.68), kind=kLoop, calls=%fused_computation.41 | loop fusion | bytes 16777216 | tf_op jit(solution)/shard_map/slice | solution.py:112
  97.1 7.6 %copy.25 = bf16[1,8,128,4,512]{2,1,4,3,0:T(8,128)(2,1)} copy(bf16[1,8,128,4,512]{4,2,0,3,1:T(8,128)(2,1)} %get-tuple-element.7) | data formatting | bytes 8388608 | tf_op jit(solution)/shard_map/slice | solution.py:112
  104.7 7.7 %copy.26 = bf16[1,8,128,4,512]{2,1,4,3,0:T(8,128)(2,1)} copy(bf16[1,8,128,4,512]{4,2,0,3,1:T(8,128)(2,1)} %get-tuple-element.8) | data formatting | bytes 8388608 | tf_op jit(solution)/shard_map/slice | solution.py:112
  112.4 3.6 %fusion.4 = f32[1024,256]{0,1:T(8,128)S(1)} fusion(bf16[256,8,8,128]{3,2,1,0:T(8,128)(2,1)} %bitcast.71, bf16[1,2048,256]{2,1,0:T(8,128)(2,1)S(1)} %copy-done), kind=kOutput, calls=%fused_computation.5 | convolution fusion | flops 1073741824 | bytes 6291456 | tf_op jit(solution)/shard_map/dot_general | solution.py:117
  116.1 1.3 fusion.6
  117.5 1.6 copy-done.1
  119.4 2.3 multiply_reduce_fusion
  121.7 8.9 %psum.7 = f32[8,1,128]{2,1,0:T(1,128)S(1)} all-reduce(f32[8,1,128]{2,1,0:T(1,128)S(1)} %bitcast.79), channel_id=1, replica_groups=mesh['ep'=8,'tp'=4] {'tp'}, use_global_device_ids=true, to_apply=%region_4.5 | all-reduce | flops 1024 | bytes 8192 | tf_op jit(solution)/shard_map/psum | solution.py:133
  130.6 8.6 %all_to_all.18 = f32[8,1,128]{2,1,0:T(1,128)S(1)} all-to-all(f32[8,1,128]{2,1,0:T(1,128)S(1)} %psum.7), channel_id=1, replica_groups=mesh['ep'=8,'tp'=4] {'ep'}, dimensions={0} | all-to-all | bytes 8192 | tf_op jit(solution)/shard_map/all_to_all | solution.py:134
  139.2 0.6 select_reduce_fusion
  139.8 7.9 %all_to_all.19 = f32[8,1,128]{2,1,0:T(1,128)S(1)} all-to-all(f32[8,1,128]{2,1,0:T(1,128)S(1)} %bitcast.78), channel_id=1, replica_groups=mesh['ep'=8,'tp'=4] {'ep'}, dimensions={0} | all-to-all | bytes 8192 | tf_op jit(solution)/shard_map/all_to_all | solution.py:115
  147.7 2.3 multiply_convert_fusion.1
  150.1 1.3 fusion.27
  151.4 3.3 %add_convert_fusion = bf16[1024,2048]{1,0:T(8,128)(2,1)} fusion(f32[1024,2048]{1,0:T(8,128)S(1)} %fusion.27, bf16[1024,256]{0,1:T(8,128)(2,1)S(1)} %get-tuple-element.9, bf16[1,2048,256]{2,1,0:T(8,128)(2,1)S(1)} %copy-done.5), kind=kOutput, calls=%fused_computation | convolution fusion | flops 1077936128 | bytes 14155776 | tf_op jit(solution)/shard_map/rf,df->rd/dot_general | solution.py:127
  155.0 49.7 %reduce-scatter.3.cloned.1.call-done = bf16[1024,512]{1,0:T(8,128)(2,1)} async-done(((bf16[1024,2048]{1,0:T(8,128)(2,1)}), bf16[1024,512]{1,0:T(8,128)(2,1)}) %reduce-scatter.3.cloned.1.call-update) | async-done | bytes 1048592 | tf_op jit(solution)/shard_map/reduce_scatter | solution.py:131
  204.7 4.9 %fusion.20 = f32[1,2048,256]{2,1,0:T(8,128)} fusion(bf16[1024,256]{0,1:T(8,128)(2,1)S(1)} %get-tuple-element.9, bf16[256,8,8,128]{3,2,1,0:T(8,128)(2,1)} %bitcast.72), kind=kOutput, calls=%fused_computation.17 | convolution fusion | flops 1073741824 | bytes 6815744 | tf_op jit(solution)/shard_map/rd,rf->df/dot_general | solution.py:129
  209.7 2.6 %fusion.17 = f32[1,2048,256]{2,1,0:T(8,128)} fusion(bf16[1024,256]{0,1:T(8,128)(2,1)S(1)} %get-tuple-element.10, bf16[256,8,8,128]{3,2,1,0:T(8,128)(2,1)S(1)} %bitcast.74), kind=kOutput, calls=%fused_computation.16 | convolution fusion | flops 1073741824 | bytes 6815744 | tf_op jit(solution)/shard_map/rd,rf->df/dot_general | solution.py:128
  212.3 0.5 copy-done.7
  212.8 0.4 copy-done.9
  213.2 2.7 %fusion.14 = f32[1,256,2048]{2,1,0:T(8,128)} fusion(bf16[256,8,8,128]{3,2,1,0:T(8,128)(2,1)S(1)} %bitcast.70, f32[1024]{0:T(1024)S(1)} %bitcast.76, f32[1024,256]{0,1:T(8,128)S(1)} %copy-done.9, f32[1024,256]{0,1:T(8,128)S(1)} %copy-done.7), kind=kOutput, calls=%fused_computation.15 | convolution fusion | flops 1075576832 | bytes 8392704 | tf_op jit(solution)/shard_map/rf,rd->fd/dot_general | solution.py:130
  215.9 24.3 %reduce-scatter.5.cloned.1.call-done = bf16[128,512]{1,0:T(8,128)(2,1)} async-done(((bf16[1024,512]{1,0:T(8,128)(2,1)}), bf16[128,512]{1,0:T(8,128)(2,1)}) %reduce-scatter.5.cloned.1.call-update) | async-done | bytes 131088 | tf_op jit(solution)/shard_map/reduce_scatter | solution.py:132
  (29 shorter events, 0.8 us)
Async XLA Ops:
  7.2 105.2 %copy-start = (bf16[1,2048,256]{2,1,0:T(8,128)(2,1)S(1)}, bf16[1,2048,256]{2,1,0:T(8,128)(2,1)}, u32[]{:S(2)}) copy-start(bf16[1,2048,256]{2,1,0:T(8,128)(2,1)} %param.11) | copy-start | bytes 3145732
  7.2 84.1 %all-gather.3.cloned.1.call-start = ((), (), s32[]{:S(2)}) async-start(), calls=%async_computation.6 | async-start | bytes 8650752 | tf_op jit(solution)/shard_map/all_gather | solution.py:110
  9.1 195.6 %reduce-scatter.3.cloned.1.call-start = ((), (), s32[]{:S(2)}) async-start(), calls=%async_computation.4 | async-start | bytes 5242880 | tf_op jit(solution)/shard_map/reduce_scatter | solution.py:131
  112.4 3.6 %copy-start.3 = (bf16[1,8,128,4,512]{2,1,4,3,0:T(8,128)(2,1)S(1)}, bf16[1,8,128,4,512]{2,1,4,3,0:T(8,128)(2,1)}, u32[]{:S(2)}) copy-start(bf16[1,8,128,4,512]{2,1,4,3,0:T(8,128)(2,1)} %copy.26) | copy-start | bytes 12582916
  112.4 3.7 %copy-start.5 = (bf16[1,2048,256]{2,1,0:T(8,128)(2,1)S(1)}, bf16[1,2048,256]{2,1,0:T(8,128)(2,1)}, u32[]{:S(2)}) copy-start(bf16[1,2048,256]{2,1,0:T(8,128)(2,1)} %param.12) | copy-start | bytes 3145732
  116.1 1.3 copy-start.6
  116.1 2.9 %copy-start.1 = (bf16[1,8,128,4,512]{2,1,4,3,0:T(8,128)(2,1)S(1)}, bf16[1,8,128,4,512]{2,1,4,3,0:T(8,128)(2,1)}, u32[]{:S(2)}) copy-start(bf16[1,8,128,4,512]{2,1,4,3,0:T(8,128)(2,1)} %copy.25) | copy-start | bytes 12582916
  116.1 3.2 %copy-start.12 = (bf16[1,256,2048]{2,1,0:T(8,128)(2,1)S(1)}, bf16[1,256,2048]{2,1,0:T(8,128)(2,1)}, u32[]{:S(2)}) copy-start(bf16[1,256,2048]{2,1,0:T(8,128)(2,1)} %param.13) | copy-start | bytes 3145732
  117.4 4.2 %copy-start.8 = (f32[1024,256]{0,1:T(8,128)}, f32[1024,256]{0,1:T(8,128)S(1)}, u32[]{:S(2)}) copy-start(f32[1024,256]{0,1:T(8,128)S(1)} %fusion.6) | copy-start | bytes 3145732
  119.4 19.8 %copy-start.10 = (s32[128,2]{0,1:T(2,128)S(1)}, s32[128,2]{0,1:T(2,128)}, u32[]{:S(2)}) copy-start(s32[128,2]{0,1:T(2,128)} %param.9) | copy-start | bytes 3076
  119.4 19.8 %copy-start.11 = (f32[128,2]{0,1:T(2,128)S(1)}, f32[128,2]{0,1:T(2,128)}, u32[]{:S(2)}) copy-start(f32[128,2]{0,1:T(2,128)} %param.10) | copy-start | bytes 3076
  154.7 85.5 %reduce-scatter.5.cloned.1.call-start = ((), (), s32[]{:S(2)}) async-start(), calls=%async_computation.5 | async-start | bytes 1179648 | tf_op jit(solution)/shard_map/reduce_scatter | solution.py:132
  204.7 5.0 %copy-start.4 = (bf16[1,8,128,4,512]{2,1,4,3,0:T(8,128)(2,1)S(1)}, bf16[1,8,128,4,512]{2,1,4,3,0:T(8,128)(2,1)}, u32[]{:S(2)}) copy-start(bf16[1,8,128,4,512]{2,1,4,3,0:T(8,128)(2,1)} %copy.26) | copy-start | bytes 12582916
  209.7 2.6 %copy-start.2 = (bf16[1,8,128,4,512]{2,1,4,3,0:T(8,128)(2,1)S(1)}, bf16[1,8,128,4,512]{2,1,4,3,0:T(8,128)(2,1)}, u32[]{:S(2)}) copy-start(bf16[1,8,128,4,512]{2,1,4,3,0:T(8,128)(2,1)} %copy.25) | copy-start | bytes 12582916
  209.7 3.1 %copy-start.7 = (f32[1024,256]{0,1:T(8,128)S(1)}, f32[1024,256]{0,1:T(8,128)}, u32[]{:S(2)}) copy-start(f32[1024,256]{0,1:T(8,128)} %copy-done.6) | copy-start | bytes 3145732
  209.7 3.5 %copy-start.9 = (f32[1024,256]{0,1:T(8,128)S(1)}, f32[1024,256]{0,1:T(8,128)}, u32[]{:S(2)}) copy-start(f32[1024,256]{0,1:T(8,128)} %copy-done.8) | copy-start | bytes 3145732
Sparse Core Ops, SparseCore 0:
  11.4 79.7 all-gather.2
  154.9 49.7 reduce-scatter.2
  207.6 32.6 reduce-scatter.4

commit v2 on v0

--- a/solution.py
+++ b/solution.py
@@ -1,6 +1,10 @@
+import functools
+
 import jax
 import jax.numpy as jnp
 from jax import lax
+from jax.experimental import pallas as pl
+from jax.experimental.pallas import tpu as pltpu
 from jax.sharding import PartitionSpec as P
 
 
@@ -11,7 +15,7 @@
     return flat_ids * capacity + jnp.sum(earlier * onehot, axis=1)
 
 
-def on_device(tokens, cotangent, routes, route_weight, w_gate, w_up, w_down):
+def slotted(tokens, cotangent, routes, route_weight, w_gate, w_up, w_down):
     f32 = jnp.float32
     tok_rows, model_width = tokens.shape
     choices_row = routes.shape[1]
@@ -98,6 +102,303 @@
     grad_route_weight = back_gate.reshape(recv_rows)[slot_ids].reshape(tok_rows, choices_row)
     grad_tokens = jnp.sum(picked, axis=1).astype(jnp.bfloat16)
     return (grad_tokens, grad_route_weight, grad_gate, grad_up, grad_down)
+
+
+def kernel(ep, tp, tokens, cotangent, table, w_gate, w_up, w_down,
+           out_tok, out_home, out_gate, out_up, out_down,
+           full, gate_v, up_v, down_v, weights, part, other, top, bottom,
+           in_top, in_bottom, last_top, last_bottom, share, arrived,
+           d_gate, d_up, act_w, g_gate, g_up, g_down, score, scores, total, home, result,
+           local, sent, got):
+    f32, bf16 = jnp.float32, jnp.bfloat16
+    rows, width = tokens.shape
+    cols = width // tp
+    half = rows // 2
+    nz = ep // 2
+    e, t = lax.axis_index("ep"), lax.axis_index("tp")
+    z, c = e // 2, lax.rem(e, 2)
+    y, x = t // 2, lax.rem(t, 2)
+    side = z * 2 + 1 - c
+    tx, ty = y * 2 + 1 - x, (1 - y) * 2 + x
+    td = (1 - y) * 2 + 1 - x
+    slots, started, locals_ = {}, [], []
+
+    def slot(*name):
+        return got.at[slots.setdefault(name, len(slots))]
+
+    def push(src, dst, name, to_e, to_t):
+        copy = pltpu.make_async_remote_copy(
+            src_ref=src, dst_ref=dst, send_sem=sent.at[len(started)], recv_sem=slot(*name),
+            device_id={"ep": to_e, "tp": to_t}, device_id_type=pl.DeviceIdType.MESH)
+        copy.start()
+        started.append(copy)
+
+    def landed(dst, *name):
+        pltpu.make_async_remote_copy(
+            src_ref=dst, dst_ref=dst, send_sem=sent.at[0], recv_sem=slot(*name),
+            device_id={"ep": side, "tp": t}, device_id_type=pl.DeviceIdType.MESH).wait_recv()
+
+    def bring(src, dst):
+        copy = pltpu.make_async_copy(src, dst, local.at[len(locals_)])
+        copy.start()
+        locals_.append(copy)
+        return copy
+
+    own = [bring(ref.at[:, pl.ds(q * cols, cols)], full.at[e, a, q])
+           for a, ref in enumerate((tokens, cotangent)) for q in range(tp)]
+    loads = [bring(w_gate.at[0], gate_v), bring(w_up.at[0], up_v), bring(w_down.at[0], down_v)]
+    weights[e] = table[...]
+
+    barrier = pltpu.get_barrier_semaphore()
+    for k in range(1, ep):
+        pl.semaphore_signal(barrier, inc=1, device_id={"ep": lax.rem(e + k, ep), "tp": t},
+                            device_id_type=pl.DeviceIdType.MESH)
+    for k in range(1, tp):
+        pl.semaphore_signal(barrier, inc=1, device_id={"ep": e, "tp": lax.rem(t + k, tp)},
+                            device_id_type=pl.DeviceIdType.MESH)
+    pl.semaphore_wait(barrier, ep + tp - 2)
+
+    def back(dz):
+        return lax.rem(z - dz + nz, nz)
+
+    for copy in own:
+        copy.wait()
+    for dz in range(1, nz):
+        for a in range(2):
+            push(full.at[e, a, t], full.at[e, a, t], ("z", dz, a), lax.rem(z + dz, nz) * 2 + c, t)
+    for a in range(2):
+        push(full.at[e, a], full.at[e, a], ("side", 0, a), side, t)
+    for k in range(1, ep):
+        push(table, weights.at[e], ("w", k), lax.rem(e + k, ep), t)
+
+    def spread(dz):
+        s = back(dz) * 2 + c
+        for a in range(2):
+            piece = full.at[s, a, t]
+            landed(piece, "z", dz, a)
+            push(piece, piece, ("x", dz, a), e, tx)
+            push(piece, piece, ("y", dz, a), e, ty)
+
+    def relay(dz):
+        s = back(dz) * 2 + c
+        piece = full.at[s, 0, ty]
+        landed(piece, "y", dz, 0)
+        push(piece, piece, ("d", dz, 0), e, tx)
+        piece = full.at[s, 1, tx]
+        landed(piece, "x", dz, 1)
+        push(piece, piece, ("d", dz, 1), e, ty)
+
+    def hand(dz):
+        s = back(dz) * 2 + c
+        landed(full.at[s, 0, tx], "x", dz, 0)
+        landed(full.at[s, 0, td], "d", dz, 0)
+        push(full.at[s, 0], full.at[s, 0], ("side", dz, 0), side, t)
+        landed(full.at[s, 1, ty], "y", dz, 1)
+        landed(full.at[s, 1, td], "d", dz, 1)
+        push(full.at[s, 1], full.at[s, 1], ("side", dz, 1), side, t)
+
+    def nt(a, b):
+        return lax.dot_general(a, b, (((1,), (1,)), ((), ())), preferred_element_type=f32)
+
+    def tn(a, b):
+        return lax.dot_general(a, b, (((0,), (0,)), ((), ())), preferred_element_type=f32)
+
+    def column(block):
+        mine = lax.broadcasted_iota(jnp.int32, (ep, rows), 0) == e
+        row = jnp.sum(jnp.where(mine, weights[block], 0.0), axis=0, keepdims=True)
+        return jnp.transpose(jnp.broadcast_to(row, (rows, rows)))[:, :1]
+
+    def compute(dz):
+        b = back(dz) * 2
+        for a in range(2):
+            landed(full.at[back(dz) * 2 + 1 - c, a], "side", dz, a)
+        g = u = bk = None
+        for q in range(tp):
+            span = pl.ds(q * cols, cols)
+            xs = jnp.concatenate([full[b, 0, q], full[b + 1, 0, q]], axis=0)
+            dy = jnp.concatenate([full[b, 1, q], full[b + 1, 1, q]], axis=0)
+            g_q = jnp.dot(xs, gate_v[span, :], preferred_element_type=f32)
+            u_q = jnp.dot(xs, up_v[span, :], preferred_element_type=f32)
+            b_q = nt(dy, down_v[:, span])
+            g, u, bk = (g_q, u_q, b_q) if q == 0 else (g + g_q, u + u_q, bk + b_q)
+        w = jnp.concatenate([column(b), column(b + 1)], axis=0)
+        sig = jax.nn.sigmoid(g)
+        silu = g * sig
+        act = silu * u
+        d_h = w * bk
+        dg = (d_h * u * sig * (1.0 + g * (1.0 - sig))).astype(bf16)
+        du = (d_h * silu).astype(bf16)
+        aw = (w * act).astype(bf16)
+        sums = jnp.sum(act * bk, axis=1, keepdims=True)
+        for i in range(2):
+            cut = slice(i * rows, (i + 1) * rows)
+            d_gate[b + i] = dg[cut]
+            d_up[b + i] = du[cut]
+            act_w[b + i] = aw[cut]
+            score[b + i] = jnp.transpose(jnp.broadcast_to(sums[cut], (rows, rows)))[:8]
+        for q in range(tp):
+            span = pl.ds(q * cols, cols)
+            piece = (nt(dg, gate_v[span, :]) + nt(du, up_v[span, :])).astype(bf16)
+            part[b, q] = piece[:rows]
+            part[b + 1, q] = piece[rows:]
+        push(part.at[back(dz) * 2 + 1 - c], other.at[dz], ("pair", dz), side, t)
+
+    for copy in loads:
+        copy.wait()
+    for k in range(1, ep):
+        landed(weights.at[lax.rem(e - k + ep, ep)], "w", k)
+    spread(1)
+    compute(0)
+    for dz in range(1, nz):
+        relay(dz)
+        if dz + 1 < nz:
+            spread(dz + 1)
+        hand(dz)
+        compute(dz)
+
+    for k in range(1, tp):
+        push(score, scores.at[t], ("score", k), e, lax.rem(t + k, tp))
+    order = list(range(1, nz)) + [0]
+
+    def add(*terms):
+        value = terms[0].astype(f32)
+        for term in terms[1:]:
+            value = value + term.astype(f32)
+        return value
+
+    def first(dz):
+        s = back(dz) * 2 + c
+        landed(other.at[dz], "pair", dz)
+        for r, q in enumerate((t, ty, tx, td)):
+            top[dz, r] = add(part[s, q, :half], other[dz, q, :half]).astype(bf16)
+        push(top.at[dz, pl.ds(2, 2)], in_top.at[dz], ("top", dz), e, tx)
+        for r, q in enumerate((t, tx, ty, td)):
+            bottom[dz, r] = add(part[s, q, half:], other[dz, q, half:]).astype(bf16)
+        push(bottom.at[dz, pl.ds(2, 2)], in_bottom.at[dz], ("bottom", dz), e, ty)
+
+    def second(dz):
+        landed(in_top.at[dz], "top", dz)
+        top[dz, 1] = add(top[dz, 1], in_top[dz, 1]).astype(bf16)
+        push(top.at[dz, 1], last_top.at[dz], ("last_top", dz), e, ty)
+        landed(in_bottom.at[dz], "bottom", dz)
+        bottom[dz, 1] = add(bottom[dz, 1], in_bottom[dz, 1]).astype(bf16)
+        push(bottom.at[dz, 1], last_bottom.at[dz], ("last_bottom", dz), e, tx)
+
+    def third(dz):
+        landed(last_top.at[dz], "last_top", dz)
+        landed(last_bottom.at[dz], "last_bottom", dz)
+        upper = add(top[dz, 0], in_top[dz, 0], last_top[dz])
+        lower = add(bottom[dz, 0], in_bottom[dz, 0], last_bottom[dz])
+        if dz:
+            share[dz - 1, :half] = upper.astype(bf16)
+            share[dz - 1, half:] = lower.astype(bf16)
+            push(share.at[dz - 1], arrived.at[dz - 1], ("share", dz), back(dz) * 2 + c, t)
+        return upper, lower
+
+    def by_width(out, ref, dst):
+        right = ref[...].reshape(ep * rows, ref.shape[2])
+        for q in range(tp):
+            out[pl.ds(q * cols, cols), :] = tn(full[:, 0, q].reshape(ep * rows, cols), right)
+        bring(out, dst.at[0])
+
+    for dz in order:
+        first(dz)
+    by_width(g_gate, d_gate, out_gate)
+    second(order[0])
+    second(order[1])
+    by_width(g_up, d_up, out_up)
+    scores[t] = score[...]
+    for k in range(1, tp):
+        landed(scores.at[lax.rem(t - k + tp, tp)], "score", k)
+    total[...] = add(*[scores[j] for j in range(tp)])
+    for k in range(1, ep):
+        to = lax.rem(e + k, ep)
+        push(total.at[to], home.at[e], ("home", k), to, t)
+    home[e] = total[e]
+    for dz in order[2:]:
+        second(dz)
+    for dz in order[:-1]:
+        third(dz)
+    left = act_w[...].reshape(ep * rows, act_w.shape[2])
+    for q in range(tp):
+        g_down[:, pl.ds(q * cols, cols)] = tn(left, full[:, 1, q].reshape(ep * rows, cols))
+    bring(g_down, out_down.at[0])
+    upper, lower = third(0)
+    for dz in range(1, nz):
+        landed(arrived.at[dz - 1], "share", dz)
+        upper = upper + arrived[dz - 1, :half].astype(f32)
+        lower = lower + arrived[dz - 1, half:].astype(f32)
+    result[:half] = upper.astype(bf16)
+    result[half:] = lower.astype(bf16)
+    bring(result, out_tok)
+    for k in range(1, ep):
+        landed(home.at[lax.rem(e - k + ep, ep)], "home", k)
+    for j in range(ep):
+        out_home[pl.ds(j, 1), :] = home[j, :1]
+    for copy in started:
+        copy.wait_send()
+    for copy in locals_[len(own) + len(loads):]:
+        copy.wait()
+
+
+def dense(tokens, cotangent, routes, route_weight, w_gate, w_up, w_down):
+    f32, bf16 = jnp.float32, jnp.bfloat16
+    rows, width = tokens.shape
+    ep, tp = lax.axis_size("ep"), lax.axis_size("tp")
+    cols, half, nz, hidden = width // tp, rows // 2, ep // 2, w_gate.shape[2]
+    hit = routes[None] == jnp.arange(ep, dtype=routes.dtype)[:, None, None]
+    table = jnp.sum(jnp.where(hit, route_weight[None], 0.0), axis=2)
+    anywhere, near = pl.BlockSpec(memory_space=pl.ANY), pl.BlockSpec(memory_space=pltpu.VMEM)
+    shape = jax.ShapeDtypeStruct
+    grad_tokens, home, gg, gu, gd = pl.pallas_call(
+        functools.partial(kernel, ep, tp),
+        out_shape=(shape((rows, cols), bf16), shape((ep, rows), f32), shape(w_gate.shape, f32),
+                   shape(w_up.shape, f32), shape(w_down.shape, f32)),
+        in_specs=[anywhere, anywhere, near, anywhere, anywhere, anywhere],
+        out_specs=(anywhere, near, anywhere, anywhere, anywhere),
+        scratch_shapes=[
+            pltpu.VMEM((ep, 2, tp, rows, cols), bf16),
+            pltpu.VMEM((width, hidden), bf16),
+            pltpu.VMEM((width, hidden), bf16),
+            pltpu.VMEM((hidden, width), bf16),
+            pltpu.VMEM((ep, ep, rows), f32),
+            pltpu.VMEM((ep, tp, rows, cols), bf16),
+            pltpu.VMEM((nz, tp, rows, cols), bf16),
+            pltpu.VMEM((nz, 4, half, cols), bf16),
+            pltpu.VMEM((nz, 4, half, cols), bf16),
+            pltpu.VMEM((nz, 2, half, cols), bf16),
+            pltpu.VMEM((nz, 2, half, cols), bf16),
+            pltpu.VMEM((nz, half, cols), bf16),
+            pltpu.VMEM((nz, half, cols), bf16),
+            pltpu.VMEM((nz - 1, rows, cols), bf16),
+            pltpu.VMEM((nz - 1, rows, cols), bf16),
+            pltpu.VMEM((ep, rows, hidden), bf16),
+            pltpu.VMEM((ep, rows, hidden), bf16),
+            pltpu.VMEM((ep, rows, hidden), bf16),
+            pltpu.VMEM((width, hidden), f32),
+            pltpu.VMEM((width, hidden), f32),
+            pltpu.VMEM((hidden, width), f32),
+            pltpu.VMEM((ep, 8, rows), f32),
+            pltpu.VMEM((tp, ep, 8, rows), f32),
+            pltpu.VMEM((ep, 8, rows), f32),
+            pltpu.VMEM((ep, 8, rows), f32),
+            pltpu.VMEM((rows, cols), bf16),
+            pltpu.SemaphoreType.DMA((16 + 2 * tp,)),
+            pltpu.SemaphoreType.DMA((24 * nz,)),
+            pltpu.SemaphoreType.DMA((24 * nz,)),
+        ],
+        compiler_params=pltpu.CompilerParams(
+            collective_id=0, has_side_effects=True, vmem_limit_bytes=50 * 1024 * 1024),
+    )(tokens, cotangent, table, w_gate, w_up, w_down)
+    grw = jnp.sum(jnp.where(hit, home[:, :, None], 0.0), axis=0)
+    return grad_tokens, grw, gg, gu, gd
+
+
+def on_device(*args):
+    rows, width = args[0].shape
+    ep, tp = lax.axis_size("ep"), lax.axis_size("tp")
+    fits = tp == 4 and ep % 2 == 0 and rows % 128 == 0 and 4 * rows * width * ep <= 1 << 24
+    return (dense if fits else slotted)(*args)
 
 
 def solution(mesh):

time: 205 us -> 113 us (0.55)
  waiting for transfers between devices: 109 us -> 0 us
  Pallas kernels: 0 us -> 98.2 us
  starting transfers between devices: 23.9 us -> 0 us
  matrix products: 18 us -> 0 us
  local copies, waits for them, and re-layouts: 26.3 us -> 12.1 us
  between operations: 14.2 us -> 0.66 us
  blocking collectives: 10 us -> 0 us
    pallas_call x0 -> x1, Pallas kernels: none -> 98.2 us  [dense(): pl.pallas_call(functools.partial(kernel, ep, tp), out_shape=(shape((rows,...]
    all_to_all x5 -> x0, waiting for transfers between devices: 94.4 us -> none  [the longest x1 45.6 us: on_device(): lax.all_to_all(send_dy.reshape(experts, capacity, model_width), 'ep', spl...]
    all_to_all x5 -> x0, starting transfers between devices: 23.7 us -> none  [the longest x1 6.35 us: on_device(): lax.all_to_all(send_w.reshape(experts, capacity, 1).astype(jnp.bfloat16),...]
    dot_general x8 -> x0, matrix products: 18 us -> none  [the longest x1 3.79 us: on_device(): jnp.einsum('rf,rd->fd', act, weighted_cot, preferred_element_type=f32)[None]]
    reduce_scatter x1 -> x0, waiting for transfers between devices: 14.8 us -> none  [on_device(): lax.psum_scatter(rounded_part.astype(jnp.bfloat16), 'tp', scatter_dimensi...]
    psum x1 -> x0, blocking collectives: 10 us -> none  [on_device(): gate_total = lax.psum(gate_part, 'tp')]
    scatter x3 -> x0, local copies, waits for them, and re-layouts: 9.51 us -> none  [the longest x1 4.4 us: on_device(): send_dy = jnp.zeros((recv_rows, model_width), jnp.bfloat16).at[slot_ids]....]
    unnamed x15 -> x18, local copies, waits for them, and re-layouts: 2.87 us -> 12.1 us
  transfers between devices with their start and end apart: 6 -> 0, of which waited for: 5 -> 0; matrix products, arithmetic and copies ran while one was open for 15% -> 0% of each run, Pallas kernels for 0% -> 0%
where the time goes in v2:
time: 113 us; the launch traced here: 112 us
  Pallas kernels  98.2 us (87%)
  local copies, waits for them, and re-layouts  12.1 us (11%)
  other arithmetic  1.28 us (1%)
    pallas_call x1, Pallas kernels, dense(): pl.pallas_call(functools.partial(kernel, ep, tp), out_shape=(shape((rows,...  98.2 us
    unnamed x18, local copies, waits for them, and re-layouts  12.1 us

profile of v2, /device:TPU:0, one launch (start us, length us, event | category | flops | bytes accessed | tf_op | source)
XLA Modules:
  0.0 112.2 jit_solution(402303614338507150)
XLA Ops:
  0.6 0.7 select_reduce_fusion.1.table
  1.3 0.0 copy-start
  1.3 1.2 %copy-done = bf16[1,2048,256]{2,1,0:T(8,128)(2,1)S(1)} copy-done((bf16[1,2048,256]{2,1,0:T(8,128)(2,1)S(1)}, bf16[1,2048,256]{2,1,0:T(8,128)(2,1)}, u32[]{:S(2)}) %copy-start) | copy-done | bytes 1048600
  2.6 0.0 copy-start.1
  2.6 1.2 %copy-done.1 = bf16[1,2048,256]{2,1,0:T(8,128)(2,1)S(1)} copy-done((bf16[1,2048,256]{2,1,0:T(8,128)(2,1)S(1)}, bf16[1,2048,256]{2,1,0:T(8,128)(2,1)}, u32[]{:S(2)}) %copy-start.1) | copy-done | bytes 1048600
  3.8 0.0 copy-start.2
  3.8 1.0 copy-done.2
  4.8 0.0 copy-start.3
  4.8 1.0 copy-done.3
  5.9 0.0 copy-start.6
  5.9 98.2 %shard_map.110 = (bf16[128,512]{1,0:T(8,128)(2,1)S(1)}, f32[8,128]{1,0:T(8,128)S(1)}, f32[1,2048,256]{2,1,0:T(8,128)}, f32[1,2048,256]{2,1,0:T(8,128)}, f32[1,256,2048]{2,1,0:T(8,128)}) custom-call(bf16[128,2048]{1,0:T(8,128)(2,1)S(1)} %copy-done.2, bf16[128,2048]{1,0:T(8,128)(2,1)S(1)} %copy-done.3, f32[8,128]{1,0:T(8,128)S(1)} %select_reduce_fusion.1.table, ...), custom_call_target="tpu_custom_call" | custom-call | tf_op jit(solution)/shard_map/pallas_call | solution.py:353
  104.1 0.0 copy-done.6
  104.1 0.6 select_reduce_fusion
  104.7 0.7 copy.18
  105.4 0.0 copy-start.5
  105.4 3.2 %copy.19 = f32[1,2048,256]{2,1,0:T(8,128)} copy(f32[1,2048,256]{2,1,0:T(8,128)} %get-tuple-element.22) | data formatting | bytes 4194304
  108.6 0.0 copy-done.5
  108.6 0.0 copy-start.4
  108.6 1.3 %copy.20 = f32[1,2048,256]{2,1,0:T(8,128)} copy(f32[1,2048,256]{2,1,0:T(8,128)S(1)} %copy-done.5) | data formatting | bytes 4194304
  109.9 1.0 copy-done.4
  110.9 1.3 %copy.21 = f32[1,256,2048]{2,1,0:T(8,128)} copy(f32[1,256,2048]{2,1,0:T(8,128)S(1)} %copy-done.4) | data formatting | bytes 4194304
Async XLA Ops:
  1.3 1.2 %copy-start = (bf16[1,2048,256]{2,1,0:T(8,128)(2,1)S(1)}, bf16[1,2048,256]{2,1,0:T(8,128)(2,1)}, u32[]{:S(2)}) copy-start(bf16[1,2048,256]{2,1,0:T(8,128)(2,1)} %w_gate.1) | copy-start | bytes 3145732
  2.6 1.2 %copy-start.1 = (bf16[1,2048,256]{2,1,0:T(8,128)(2,1)S(1)}, bf16[1,2048,256]{2,1,0:T(8,128)(2,1)}, u32[]{:S(2)}) copy-start(bf16[1,2048,256]{2,1,0:T(8,128)(2,1)} %w_up.1) | copy-start | bytes 3145732
  3.8 1.0 copy-start.2
  4.8 1.0 copy-start.3
  5.9 98.3 %copy-start.6 = (s32[128,2]{0,1:T(2,128)S(1)}, s32[128,2]{0,1:T(2,128)}, u32[]{:S(2)}) copy-start(s32[128,2]{0,1:T(2,128)} %param.9) | copy-start | bytes 3076
  105.4 3.2 %copy-start.5 = (f32[1,2048,256]{2,1,0:T(8,128)S(1)}, f32[1,2048,256]{2,1,0:T(8,128)}, u32[]{:S(2)}) copy-start(f32[1,2048,256]{2,1,0:T(8,128)} %get-tuple-element.23) | copy-start | bytes 6291460
  108.6 2.3 %copy-start.4 = (f32[1,256,2048]{2,1,0:T(8,128)S(1)}, f32[1,256,2048]{2,1,0:T(8,128)}, u32[]{:S(2)}) copy-start(f32[1,256,2048]{2,1,0:T(8,128)} %get-tuple-element.24) | copy-start | bytes 6291460

commit v3 on v2

--- a/solution.py
+++ b/solution.py
@@ -158,14 +158,28 @@
                             device_id_type=pl.DeviceIdType.MESH)
     pl.semaphore_wait(barrier, ep + tp - 2)
 
-    def back(dz):
-        return lax.rem(z - dz + nz, nz)
+    edge = jnp.minimum(z, nz - 1 - z)
+
+    def back(i):
+        near = z + (i + 1) // 2 * (1 - i % 2 * 2)
+        away = jnp.where(z < nz - 1 - z, z + i - edge, z - i + edge)
+        return jnp.where(i <= 2 * edge, near, away) if i else z
+
+    relays = []
+
+    def along(piece, from_z, a, go, to_z):
+        copy = pltpu.make_async_remote_copy(
+            src_ref=piece, dst_ref=piece, send_sem=sent.at[20 * nz + len(relays)],
+            recv_sem=got.at[20 * nz + from_z * 2 + a],
+            device_id={"ep": to_z * 2 + c, "tp": t}, device_id_type=pl.DeviceIdType.MESH)
+        pl.when(go)(copy.start)
+        relays.append((go, copy))
 
     for copy in own:
         copy.wait()
-    for dz in range(1, nz):
-        for a in range(2):
-            push(full.at[e, a, t], full.at[e, a, t], ("z", dz, a), lax.rem(z + dz, nz) * 2 + c, t)
+    for a in range(2):
+        along(full.at[e, a, t], z, a, z < nz - 1, jnp.minimum(z + 1, nz - 1))
+        along(full.at[e, a, t], z, a, z > 0, jnp.maximum(z - 1, 0))
     for a in range(2):
         push(full.at[e, a], full.at[e, a], ("side", 0, a), side, t)
     for k in range(1, ep):
@@ -175,7 +189,14 @@
         s = back(dz) * 2 + c
         for a in range(2):
             piece = full.at[s, a, t]
-            landed(piece, "z", dz, a)
+            pltpu.make_async_remote_copy(
+                src_ref=piece, dst_ref=piece, send_sem=sent.at[0],
+                recv_sem=got.at[20 * nz + back(dz) * 2 + a],
+                device_id={"ep": side, "tp": t}, device_id_type=pl.DeviceIdType.MESH).wait_recv()
+            below = back(dz) < z
+            go = jnp.where(below, z < nz - 1, z > 0)
+            onward = jnp.where(below, jnp.minimum(z + 1, nz - 1), jnp.maximum(z - 1, 0))
+            along(piece, back(dz), a, go, onward)
             push(piece, piece, ("x", dz, a), e, tx)
             push(piece, piece, ("y", dz, a), e, ty)
 
@@ -247,18 +268,6 @@
         copy.wait()
     for k in range(1, ep):
         landed(weights.at[lax.rem(e - k + ep, ep)], "w", k)
-    spread(1)
-    compute(0)
-    for dz in range(1, nz):
-        relay(dz)
-        if dz + 1 < nz:
-            spread(dz + 1)
-        hand(dz)
-        compute(dz)
-
-    for k in range(1, tp):
-        push(score, scores.at[t], ("score", k), e, lax.rem(t + k, tp))
-    order = list(range(1, nz)) + [0]
 
     def add(*terms):
         value = terms[0].astype(f32)
@@ -292,7 +301,12 @@
         if dz:
             share[dz - 1, :half] = upper.astype(bf16)
             share[dz - 1, half:] = lower.astype(bf16)
-            push(share.at[dz - 1], arrived.at[dz - 1], ("share", dz), back(dz) * 2 + c, t)
+            copy = pltpu.make_async_remote_copy(
+                src_ref=share.at[dz - 1], dst_ref=arrived.at[z], send_sem=sent.at[len(started)],
+                recv_sem=got.at[22 * nz + z], device_id={"ep": back(dz) * 2 + c, "tp": t},
+                device_id_type=pl.DeviceIdType.MESH)
+            copy.start()
+            started.append(copy)
         return upper, lower
 
     def by_width(out, ref, dst):
@@ -301,13 +315,30 @@
             out[pl.ds(q * cols, cols), :] = tn(full[:, 0, q].reshape(ep * rows, cols), right)
         bring(out, dst.at[0])
 
-    for dz in order:
-        first(dz)
+    spread(1)
+    compute(0)
+    if nz > 2:
+        spread(2)
+    for dz in range(1, nz):
+        relay(dz)
+        if dz + 2 < nz:
+            spread(dz + 2)
+        if dz > 1:
+            second(dz - 2)
+        first(dz - 1)
+        hand(dz)
+        compute(dz)
+    for k in range(1, tp):
+        push(score, scores.at[t], ("score", k), e, lax.rem(t + k, tp))
+    scores[t] = score[...]
+    for dz in range(1, nz - 2):
+        third(dz)
+    second(nz - 2)
+    first(nz - 1)
     by_width(g_gate, d_gate, out_gate)
-    second(order[0])
-    second(order[1])
-    by_width(g_up, d_up, out_up)
-    scores[t] = score[...]
+    for dz in range(max(1, nz - 2), nz - 1):
+        third(dz)
+    second(nz - 1)
     for k in range(1, tp):
         landed(scores.at[lax.rem(t - k + tp, tp)], "score", k)
     total[...] = add(*[scores[j] for j in range(tp)])
@@ -315,19 +346,21 @@
         to = lax.rem(e + k, ep)
         push(total.at[to], home.at[e], ("home", k), to, t)
     home[e] = total[e]
-    for dz in order[2:]:
-        second(dz)
-    for dz in order[:-1]:
-        third(dz)
+    by_width(g_up, d_up, out_up)
+    third(nz - 1)
     left = act_w[...].reshape(ep * rows, act_w.shape[2])
     for q in range(tp):
         g_down[:, pl.ds(q * cols, cols)] = tn(left, full[:, 1, q].reshape(ep * rows, cols))
     bring(g_down, out_down.at[0])
     upper, lower = third(0)
-    for dz in range(1, nz):
-        landed(arrived.at[dz - 1], "share", dz)
-        upper = upper + arrived[dz - 1, :half].astype(f32)
-        lower = lower + arrived[dz - 1, half:].astype(f32)
+    for k in range(1, nz):
+        j = lax.rem(z + k, nz)
+        pltpu.make_async_remote_copy(
+            src_ref=arrived.at[j], dst_ref=arrived.at[j], send_sem=sent.at[0],
+            recv_sem=got.at[22 * nz + j], device_id={"ep": side, "tp": t},
+            device_id_type=pl.DeviceIdType.MESH).wait_recv()
+        upper = upper + arrived[j, :half].astype(f32)
+        lower = lower + arrived[j, half:].astype(f32)
     result[:half] = upper.astype(bf16)
     result[half:] = lower.astype(bf16)
     bring(result, out_tok)
@@ -335,8 +368,11 @@
         landed(home.at[lax.rem(e - k + ep, ep)], "home", k)
     for j in range(ep):
         out_home[pl.ds(j, 1), :] = home[j, :1]
+    assert len(started) <= 20 * nz and len(slots) <= 20 * nz and len(relays) <= 4 * nz
     for copy in started:
         copy.wait_send()
+    for go, copy in relays:
+        pl.when(go)(copy.wait_send)
     for copy in locals_[len(own) + len(loads):]:
         copy.wait()
 
@@ -348,7 +384,7 @@
     cols, half, nz, hidden = width // tp, rows // 2, ep // 2, w_gate.shape[2]
     hit = routes[None] == jnp.arange(ep, dtype=routes.dtype)[:, None, None]
     table = jnp.sum(jnp.where(hit, route_weight[None], 0.0), axis=2)
-    anywhere, near = pl.BlockSpec(memory_space=pl.ANY), pl.BlockSpec(memory_space=pltpu.VMEM)
+    anywhere, near = pl.BlockSpec(memory_space=pltpu.HBM), pl.BlockSpec(memory_space=pltpu.VMEM)
     shape = jax.ShapeDtypeStruct
     grad_tokens, home, gg, gu, gd = pl.pallas_call(
         functools.partial(kernel, ep, tp),
@@ -371,7 +407,7 @@
             pltpu.VMEM((nz, half, cols), bf16),
             pltpu.VMEM((nz, half, cols), bf16),
             pltpu.VMEM((nz - 1, rows, cols), bf16),
-            pltpu.VMEM((nz - 1, rows, cols), bf16),
+            pltpu.VMEM((nz, rows, cols), bf16),
             pltpu.VMEM((ep, rows, hidden), bf16),
             pltpu.VMEM((ep, rows, hidden), bf16),
             pltpu.VMEM((ep, rows, hidden), bf16),

time: 113 us -> 90.8 us (0.80)
  Pallas kernels: 98.2 us -> 76.5 us
    pallas_call x1, Pallas kernels: 98.2 us -> 76.5 us  [dense(): pl.pallas_call(functools.partial(kernel, ep, tp), out_shape=(shape((rows,...]
where the time goes in v3:
time: 90.8 us; the launch traced here: 90.4 us
  Pallas kernels  76.5 us (84%)
  local copies, waits for them, and re-layouts  12.1 us (13%)
  other arithmetic  1.28 us (1%)
    pallas_call x1, Pallas kernels, dense(): pl.pallas_call(functools.partial(kernel, ep, tp), out_shape=(shape((rows,...  76.5 us
    unnamed x18, local copies, waits for them, and re-layouts  12.1 us

profile of v3, /device:TPU:0, one launch (start us, length us, event | category | flops | bytes accessed | tf_op | source)
XLA Modules:
  0.0 90.4 jit_solution(17298228571536511358)
XLA Ops:
  0.6 0.7 select_reduce_fusion.1.table
  1.3 0.0 copy-start
  1.3 1.2 %copy-done = bf16[1,2048,256]{2,1,0:T(8,128)(2,1)S(1)} copy-done((bf16[1,2048,256]{2,1,0:T(8,128)(2,1)S(1)}, bf16[1,2048,256]{2,1,0:T(8,128)(2,1)}, u32[]{:S(2)}) %copy-start) | copy-done | bytes 1048600
  2.6 0.0 copy-start.1
  2.6 1.2 %copy-done.1 = bf16[1,2048,256]{2,1,0:T(8,128)(2,1)S(1)} copy-done((bf16[1,2048,256]{2,1,0:T(8,128)(2,1)S(1)}, bf16[1,2048,256]{2,1,0:T(8,128)(2,1)}, u32[]{:S(2)}) %copy-start.1) | copy-done | bytes 1048600
  3.8 0.0 copy-start.2
  3.8 1.0 %copy-done.2 = bf16[128,2048]{1,0:T(8,128)(2,1)S(1)} copy-done((bf16[128,2048]{1,0:T(8,128)(2,1)S(1)}, bf16[128,2048]{1,0:T(8,128)(2,1)}, u32[]{:S(2)}) %copy-start.2) | copy-done | bytes 524312
  4.8 0.0 copy-start.3
  4.8 1.0 %copy-done.3 = bf16[128,2048]{1,0:T(8,128)(2,1)S(1)} copy-done((bf16[128,2048]{1,0:T(8,128)(2,1)S(1)}, bf16[128,2048]{1,0:T(8,128)(2,1)}, u32[]{:S(2)}) %copy-start.3) | copy-done | bytes 524312
  5.9 0.0 copy-start.6
  5.9 76.5 %shard_map.110 = (bf16[128,512]{1,0:T(8,128)(2,1)S(1)}, f32[8,128]{1,0:T(8,128)S(1)}, f32[1,2048,256]{2,1,0:T(8,128)}, f32[1,2048,256]{2,1,0:T(8,128)}, f32[1,256,2048]{2,1,0:T(8,128)}) custom-call(bf16[128,2048]{1,0:T(8,128)(2,1)S(1)} %copy-done.2, bf16[128,2048]{1,0:T(8,128)(2,1)S(1)} %copy-done.3, f32[8,128]{1,0:T(8,128)S(1)} %select_reduce_fusion.1.table, ...), custom_call_target="tpu_custom_call" | custom-call | tf_op jit(solution)/shard_map/pallas_call | solution.py:389
  82.3 0.0 copy-done.6
  82.3 0.6 select_reduce_fusion
  82.9 0.7 copy.18
  83.6 0.0 copy-start.5
  83.6 3.2 %copy.19 = f32[1,2048,256]{2,1,0:T(8,128)} copy(f32[1,2048,256]{2,1,0:T(8,128)} %get-tuple-element.22) | data formatting | bytes 4194304
  86.8 0.0 copy-done.5
  86.8 0.0 copy-start.4
  86.8 1.3 %copy.20 = f32[1,2048,256]{2,1,0:T(8,128)} copy(f32[1,2048,256]{2,1,0:T(8,128)S(1)} %copy-done.5) | data formatting | bytes 4194304
  88.1 1.0 %copy-done.4 = f32[1,256,2048]{2,1,0:T(8,128)S(1)} copy-done((f32[1,256,2048]{2,1,0:T(8,128)S(1)}, f32[1,256,2048]{2,1,0:T(8,128)}, u32[]{:S(2)}) %copy-start.4) | copy-done | bytes 2097176
  89.1 1.3 %copy.21 = f32[1,256,2048]{2,1,0:T(8,128)} copy(f32[1,256,2048]{2,1,0:T(8,128)S(1)} %copy-done.4) | data formatting | bytes 4194304
Async XLA Ops:
  1.3 1.2 %copy-start = (bf16[1,2048,256]{2,1,0:T(8,128)(2,1)S(1)}, bf16[1,2048,256]{2,1,0:T(8,128)(2,1)}, u32[]{:S(2)}) copy-start(bf16[1,2048,256]{2,1,0:T(8,128)(2,1)} %w_gate.1) | copy-start | bytes 3145732
  2.6 1.2 %copy-start.1 = (bf16[1,2048,256]{2,1,0:T(8,128)(2,1)S(1)}, bf16[1,2048,256]{2,1,0:T(8,128)(2,1)}, u32[]{:S(2)}) copy-start(bf16[1,2048,256]{2,1,0:T(8,128)(2,1)} %w_up.1) | copy-start | bytes 3145732
  3.8 1.0 %copy-start.2 = (bf16[128,2048]{1,0:T(8,128)(2,1)S(1)}, bf16[128,2048]{1,0:T(8,128)(2,1)}, u32[]{:S(2)}) copy-start(bf16[128,2048]{1,0:T(8,128)(2,1)} %tokens.1) | copy-start | bytes 1572868
  4.8 1.0 %copy-start.3 = (bf16[128,2048]{1,0:T(8,128)(2,1)S(1)}, bf16[128,2048]{1,0:T(8,128)(2,1)}, u32[]{:S(2)}) copy-start(bf16[128,2048]{1,0:T(8,128)(2,1)} %cotangent.1) | copy-start | bytes 1572868
  5.9 76.5 %copy-start.6 = (s32[128,2]{0,1:T(2,128)S(1)}, s32[128,2]{0,1:T(2,128)}, u32[]{:S(2)}) copy-start(s32[128,2]{0,1:T(2,128)} %param.9) | copy-start | bytes 3076
  83.6 3.2 %copy-start.5 = (f32[1,2048,256]{2,1,0:T(8,128)S(1)}, f32[1,2048,256]{2,1,0:T(8,128)}, u32[]{:S(2)}) copy-start(f32[1,2048,256]{2,1,0:T(8,128)} %get-tuple-element.23) | copy-start | bytes 6291460
  86.8 2.3 %copy-start.4 = (f32[1,256,2048]{2,1,0:T(8,128)S(1)}, f32[1,256,2048]{2,1,0:T(8,128)}, u32[]{:S(2)}) copy-start(f32[1,256,2048]{2,1,0:T(8,128)} %get-tuple-element.24) | copy-start | bytes 6291460
